TPU v7x, 32 devices: a whole 2x2x4 slice. The times are simulated.
32 devices in a mesh: sp: 8 (over z, y), tp: 4 (over x, core).
Axes of the slice: x: 2, y: 2, z: 4, core: 2. Of those that a mesh axis runs over, the one named last changes fastest.
Arguments:
- resid_stream: bfloat16 [3072, 2048], P('sp'), may hold values from -6 to 6
- q_latent: bfloat16 [3072, 512], P('sp'), may hold values from -6 to 6
- kv_latent: bfloat16 [3072, 256], P('sp'), may hold values from -6 to 6
- rope_key: bfloat16 [3072, 64], P('sp'), may hold values from -6 to 6
- doc_ids: int32 [3072], P('sp'), may hold values from 0 to 3, as said below
- q_gain: float32 [512], replicated, may hold values from 1.5 to 64
- kv_gain: float32 [256], replicated, may hold values from 0.1 to 1.9
- w_query: bfloat16 [512, 3072], P(None, 'tp'), may hold values from -0.25 to 0.25
- w_key: bfloat16 [256, 2048], P(None, 'tp'), may hold values from -0.375 to 0.375
- w_value: bfloat16 [256, 2048], P(None, 'tp'), may hold values from -0.375 to 0.375
- w_out: bfloat16 [2048, 2048], replicated, may hold values from -0.5 to 0.5
- mix_gain: float32 [2048], replicated, may hold values from 0.1 to 1.9
- w_gate: bfloat16 [2048, 5632], P('sp', 'tp'), may hold values from -0.125 to 0.125
- w_up: bfloat16 [2048, 5632], P('sp', 'tp'), may hold values from -0.125 to 0.125
- w_down: bfloat16 [5632, 2048], P('tp', 'sp'), may hold values from -0.3125 to 0.3125
- out_gain: float32 [2048], replicated, may hold values from 0.1 to 1.9
Outputs:
- layer_out: bfloat16 [3072, 2048], P(('sp', 'tp'))
Inputs may be any that keep to these rules, and one draw needn't show every extreme that they name: `doc_ids`: document numbers never fall along the sequence; every document has 1 to 2304 positions and one has exactly 2304.
All inputs are finite; a program needn't handle non-finite values.
Results may differ from a plain program's by a relative error of at most 0.02.
The roundings to bfloat16 on the way count: a program that leaves them out, or rounds other values in their place, can miss the bound.
Values may be sent and summed in bfloat16 or wider, within the bound.
No kernel may reach another device: no remote copies, remote signals or barrier semaphores. Data moves between devices by JAX's collectives and lax.ppermute only.
A program may use at most 128 MiB of HBM per device.

v0:
```python
import jax
import jax.numpy as jnp
from jax import lax
from jax.sharding import PartitionSpec as P

NOPE = 128
RD = 64
VD = 128


eps_norm = 1e-05
rope_theta = 10000.0
resid_alpha = 8.0**0.25
key_span = 2048


def rope_angles(positions):
    frequency = rope_theta ** (-jnp.arange(0, RD, 2, dtype=jnp.float32) / RD)
    angles = positions.astype(jnp.float32)[:, None] * frequency[None, :]
    return (jnp.cos(angles), jnp.sin(angles))


def rotate(values, cos_table, sin_table):
    half_width = values.shape[-1] // 2
    first_half = values[..., :half_width]
    second_half = values[..., half_width:]
    return jnp.concatenate(
        [
            first_half * cos_table - second_half * sin_table,
            second_half * cos_table + first_half * sin_table,
        ],
        axis=-1,
    )


def rms_scaled(latent, scaling):
    widened = latent.astype(jnp.float32)
    inverse = lax.rsqrt(jnp.mean(widened * widened, axis=-1, keepdims=True) + eps_norm)
    return (widened * inverse * scaling).astype(jnp.bfloat16)


def layer_scaled(stream, scaling):
    centre = stream - jnp.mean(stream, axis=-1, keepdims=True)
    spread = jnp.mean(centre * centre, axis=-1, keepdims=True)
    return centre * lax.rsqrt(spread + eps_norm) * scaling


def fold_in_blocks(carried, piece_part, attend_fn):
    piece_rows = piece_part[0].shape[0]
    if piece_rows > key_span and piece_rows % key_span == 0:

        def one_block(inner, block_index):
            sliced = tuple(
                (
                    lax.dynamic_slice_in_dim(
                        member, (block_index * key_span).astype(jnp.int32), key_span, 0
                    )
                    for member in piece_part
                )
            )
            return (attend_fn(inner, sliced), None)

        outcome = lax.scan(one_block, carried, jnp.arange(piece_rows // key_span, dtype=jnp.int32))
        return outcome[0]
    return attend_fn(carried, piece_part)


def body(
    resid_stream,
    q_latent,
    kv_latent,
    rope_key,
    doc_ids,
    q_gain,
    kv_gain,
    w_query,
    w_key,
    w_value,
    w_out,
    mix_gain,
    w_gate,
    w_up,
    w_down,
    out_gain,
):
    tok_rows = q_latent.shape[0]
    head_count = w_key.shape[1] // NOPE
    tp_count = lax.axis_size("tp")
    part_rows = tok_rows // tp_count
    tp_index = lax.axis_index("tp")
    positions = lax.axis_index("sp") * tok_rows + jnp.arange(tok_rows, dtype=jnp.int32)
    cos_table, sin_table = rope_angles(positions)
    q_normed = rms_scaled(q_latent, q_gain)
    queries = jnp.dot(q_normed, w_query, preferred_element_type=jnp.float32).reshape(
        tok_rows, head_count, NOPE + RD
    )
    query_nope = queries[:, :, :NOPE].astype(jnp.bfloat16)
    query_rope = rotate(queries[:, :, NOPE:], cos_table[:, None, :], sin_table[:, None, :]).astype(
        jnp.bfloat16
    )
    kv_normed = rms_scaled(kv_latent, kv_gain)
    key_rot = rotate(rope_key.astype(jnp.float32), cos_table, sin_table).astype(jnp.bfloat16)
    score_scale = (NOPE + RD) ** (-0.5)

    def attend_rows(carried, piece_part):
        row_top, denom_sum, accum_out = carried
        key_piece, value_piece, rot_piece, doc_piece = piece_part
        piece_rows = key_piece.shape[0]
        keys_heads = key_piece.reshape(piece_rows, head_count, NOPE)
        values_heads = value_piece.reshape(piece_rows, head_count, VD)
        scores = jnp.einsum(
            "qhd,khd->hqk", query_nope, keys_heads, preferred_element_type=jnp.float32
        )
        scores = (
            scores
            + jnp.einsum("qhd,kd->hqk", query_rope, rot_piece, preferred_element_type=jnp.float32)
        ) * score_scale
        same_doc = (doc_ids[:, None] == doc_piece[None, :])[None]
        masked = jnp.where(same_doc, scores, -1e30)
        new_top = jnp.maximum(row_top, jnp.max(masked, axis=-1))
        weights = jnp.where(same_doc, jnp.exp(masked - new_top[:, :, None]), 0.0)
        factor = jnp.exp(row_top - new_top)
        denom_sum = denom_sum * factor + jnp.sum(weights, axis=-1)
        update = jnp.einsum(
            "hqk,khd->qhd",
            weights.astype(jnp.bfloat16),
            values_heads,
            preferred_element_type=jnp.float32,
        )
        accum_out = accum_out * jnp.transpose(factor)[:, :, None] + update
        return (new_top, denom_sum, accum_out)

    initial = (
        jnp.full((head_count, tok_rows), -1e30, jnp.float32),
        jnp.zeros((head_count, tok_rows), jnp.float32),
        jnp.zeros((tok_rows, head_count, VD), jnp.float32),
    )

    def project_rows(carried, piece_part):
        latent_piece, rot_piece, doc_piece = piece_part
        key_piece = jnp.dot(latent_piece, w_key, preferred_element_type=jnp.float32).astype(
            jnp.bfloat16
        )
        value_piece = jnp.dot(latent_piece, w_value, preferred_element_type=jnp.float32).astype(
            jnp.bfloat16
        )
        return attend_rows(carried, (key_piece, value_piece, rot_piece, doc_piece))

    carried_out = fold_in_blocks(
        initial,
        (
            lax.all_gather(kv_normed, "sp", axis=0, tiled=True),
            lax.all_gather(key_rot, "sp", axis=0, tiled=True),
            lax.all_gather(doc_ids, "sp", axis=0, tiled=True),
        ),
        project_rows,
    )
    denom_sum = carried_out[1]
    attended = (
        (carried_out[2] / jnp.transpose(denom_sum)[:, :, None])
        .astype(jnp.bfloat16)
        .reshape(tok_rows, head_count * VD)
    )
    heads_rows = lax.all_to_all(attended, "tp", split_axis=0, concat_axis=1, tiled=True)
    mixer_out = jnp.dot(heads_rows, w_out, preferred_element_type=jnp.float32)
    own_resid = lax.dynamic_slice_in_dim(resid_stream, tp_index * part_rows, part_rows, 0)
    own_normed = layer_scaled(
        resid_alpha * own_resid.astype(jnp.float32) + mixer_out, mix_gain
    ).astype(jnp.bfloat16)
    normed_rows = lax.all_gather(own_normed, "tp", axis=0, tiled=True)
    gate_part = jnp.dot(
        normed_rows,
        lax.all_gather(w_gate, "sp", axis=0, tiled=True),
        preferred_element_type=jnp.float32,
    )
    up_part = jnp.dot(
        normed_rows,
        lax.all_gather(w_up, "sp", axis=0, tiled=True),
        preferred_element_type=jnp.float32,
    )
    hidden = (jax.nn.silu(gate_part) * up_part).astype(jnp.bfloat16)
    down_term = jnp.dot(
        hidden, lax.all_gather(w_down, "sp", axis=1, tiled=True), preferred_element_type=jnp.float32
    )
    ffn_sum = lax.psum_scatter(
        down_term.astype(jnp.bfloat16), "tp", scatter_dimension=0, tiled=True
    ).astype(jnp.float32)
    layer_out = layer_scaled(
        resid_alpha * own_normed.astype(jnp.float32) + 0.5 * ffn_sum, out_gain
    ).astype(jnp.bfloat16)
    return layer_out


def solution(mesh):
    in_specs = (
        P("sp", None),
        P("sp", None),
        P("sp", None),
        P("sp", None),
        P("sp"),
        P(),
        P(),
        P(None, "tp"),
        P(None, "tp"),
        P(None, "tp"),
        P(),
        P(),
        P("sp", "tp"),
        P("sp", "tp"),
        P("tp", "sp"),
        P(),
    )
    out_specs = P(("sp", "tp"), None)
    return jax.shard_map(body, mesh=mesh, in_specs=in_specs, out_specs=out_specs, check_vma=False)
```

profile of v0, /device:TPU:0, one launch (start us, length us, event | category | flops | bytes accessed | tf_op | source)
XLA Modules:
  0.0 487.2 jit_solution(11520643036253584039)
XLA Ops:
  6.5 0.0 copy-start
  6.5 0.0 copy-start.7
  6.5 0.0 all-gather.7.cloned.1.call-start
  6.5 1.1 fusion.26
  7.7 1.7 fusion.28
  9.4 0.0 all-gather.7.cloned.1.call-update
  9.5 0.8 convert_element_type.64
  10.3 0.7 reshape.152
  11.0 27.9 %all-gather = s32[8,1,384]{2,1,0:T(1,128)S(1)} all-gather(s32[1,1,384]{2,1,0:T(1,128)S(1)} %reshape.152), channel_id=1, replica_groups=mesh['sp'=8,'tp'=4] {'sp'}, dimensions={0}, use_global_device_ids=true | all-gather | bytes 13824 | tf_op jit(solution)/shard_map/all_gather | solution.py:154
  38.9 0.3 multiply_cosine_fusion
  39.2 1.2 fusion.22
  40.3 32.1 %all_gather.23 = bf16[3072,64]{0,1:T(8,128)(2,1)S(1)} all-gather(bf16[384,64]{0,1:T(8,128)(2,1)S(1)} %pad_maximum_fusion), channel_id=1, replica_groups=mesh['sp'=8,'tp'=4] {'sp'}, dimensions={0}, use_global_device_ids=true | all-gather | bytes 442368 | tf_op jit(solution)/shard_map/all_gather | solution.py:153
  72.5 0.0 copy-done
  72.5 1.7 fusion.29
  74.2 0.1 subtract_convert_fusion
  74.2 0.0 copy-done.7
  74.2 0.7 broadcast_compare_fusion
  74.9 0.0 copy-start.3
  74.9 8.1 %fusion.31 = f32[3072,384,4]{0,1,2:T(8,128)} fusion(bf16[3072,64]{0,1:T(8,128)(2,1)S(1)} %all_gather.23, bf16[384,4,32]{0,2,1:T(8,128)(2,1)S(1)} %get-tuple-element.6, bf16[384,4,32]{0,2,1:T(8,128)(2,1)S(1)} %get-tuple-element.5), kind=kOutput, calls=%fused_computation.39 | convolution fusion | flops 604372992 | bytes 19464192 | tf_op jit(solution)/shard_map/qhd,kd->hqk/dot_general | solution.py:116
  83.0 0.0 all-gather.7.cloned.1.call-done
  83.0 0.0 copy-done.3
  83.0 2.4 convolution_convert_fusion.1
  85.5 12.7 %fusion.41 = (f32[4,384]{1,0:T(4,128)S(1)}, f32[4,384,3072]{2,1,0:T(8,128)}) fusion(f32[3072,384,4]{0,1,2:T(8,128)} %fusion.31, bf16[3072,4,128]{0,2,1:T(8,128)(2,1)S(1)} %bitcast.44, f32[384,4,192]{0,2,1:T(8,128)S(1)} %bitcast.47, pred[384,3072]{1,0:T(8,128)(4,1)S(1)} %broadcast_compare_fusion), kind=kOutput, calls=%fused_computation.67 | convolution fusion | flops 1226832384 | bytes 42473472 | tf_op jit(solution)/shard_map/qhd,khd->hqk/dot_general | solution.py:111
  98.2 0.0 copy-start.2
  98.2 0.0 copy-start.4
  98.2 9.0 %fusion.2 = f32[4,384]{1,0:T(4,128)S(1)} fusion(f32[4,384,3072]{2,1,0:T(8,128)} %get-tuple-element.16, f32[4,384]{1,0:T(4,128)S(1)} %get-tuple-element.10, pred[384,3072]{1,0:T(8,128)(4,1)S(1)} %broadcast_compare_fusion), kind=kLoop, calls=%fused_computation.4 | loop fusion | flops 14154240 | bytes 20066304 | tf_op jit(solution)/shard_map/reduce_sum | solution.py:123
  107.2 0.0 copy-done.2
  107.2 0.0 copy-done.4
  107.2 2.7 convolution_convert_fusion
  109.9 10.9 %fusion.19 = bf16[384,4,128]{0,2,1:T(8,128)(2,1)S(1)} fusion(bf16[3072,4,128]{0,2,1:T(8,128)(2,1)} %bitcast.45, f32[4,384,3072]{2,1,0:T(8,128)} %get-tuple-element.16, f32[4,384]{1,0:T(4,128)S(1)} %get-tuple-element.10, pred[384,3072]{1,0:T(8,128)(4,1)S(1)} %broadcast_compare_fusion, f32[384,4]{0,1:T(4,128)S(1)} %bitcast_add_fusion.1, ...), kind=kOutput, calls=%fused_computation.22 | convolution fusion | flops 1222705152 | bytes 23611392 | tf_op jit(solution)/shard_map/hqk,khd->qhd/dot_general | solution.py:124
  120.8 0.2 copy.38
  121.1 0.9 all_to_all.14
  122.0 3.5 all-to-all-start
  125.4 0.3 all-gather.9.cloned.1.call-start
  125.7 7.1 %all-to-all-done = bf16[4,96,512]{2,1,0:T(8,128)(2,1)S(1)} async-done(((bf16[4,96,512]{2,1,0:T(8,128)(2,1)}), bf16[4,96,512]{2,1,0:T(8,128)(2,1)S(1)}, u32[]{:S(2)}, u32[]{:S(2)}) %all-to-all-start) | async-done | bytes 393248 | tf_op jit(solution)/shard_map/all_to_all | solution.py:164
  132.8 0.0 copy-start.5
  132.9 5.0 %fusion.42 = (f32[96]{0:T(128)S(1)}, f32[96,2048]{1,0:T(8,128)S(1)}) fusion(bf16[96,2048]{1,0:T(8,128)(2,1)S(1)} %bitcast.48, bf16[2048,2048]{1,0:T(8,128)(2,1)} %param.26, bf16[384,2048]{1,0:T(8,128)(2,1)} %param.16, s32[]{:T(128)S(6)} %select_n.10), kind=kOutput, calls=%fused_computation.68 | convolution fusion | flops 806092672 | bytes 9961860 | tf_op jit(solution)/shard_map/dot_general | solution.py:165
  137.8 0.2 multiply_reduce_fusion.1
  138.1 0.0 copy-done.5
  138.1 0.9 multiply_convert_fusion.1
  139.0 0.0 all-gather.9.cloned.1.call-update
  139.1 0.0 all-gather.11.cloned.1.call-start
  139.1 0.7 all-gather.11.cloned.1.call-update
  139.8 0.0 all-gather.13.cloned.1.call-start
  139.8 0.5 all-gather.13.cloned.1.call-update
  140.4 0.0 all-gather.15.cloned.1.call-start
  140.4 0.5 all-gather.15.cloned.1.call-update
  141.0 0.0 reduce-scatter.2.cloned.1.call-start
  141.0 16.3 %all-gather.9.cloned.1.call-done = bf16[384,2048]{1,0:T(8,128)(2,1)} async-done(((bf16[96,2048]{1,0:T(8,128)(2,1)}), bf16[384,2048]{1,0:T(8,128)(2,1)}) %all-gather.9.cloned.1.call-update) | async-done | bytes 1572880 | tf_op jit(solution)/shard_map/all_gather | solution.py:170
  157.3 0.0 copy-start.8
  157.3 94.5 %all-gather.11.cloned.1.call-done = bf16[2048,1408]{1,0:T(8,128)(2,1)} async-done(((bf16[256,1408]{1,0:T(8,128)(2,1)}), bf16[2048,1408]{1,0:T(8,128)(2,1)}) %all-gather.11.cloned.1.call-update) | async-done | bytes 5767184 | tf_op jit(solution)/shard_map/all_gather | solution.py:173
  251.8 7.1 %fusion.43 = f32[384,1408]{1,0:T(8,128)} fusion(bf16[384,2048]{1,0:T(8,128)(2,1)} %all-gather.9.cloned.1.call-done, bf16[2048,1408]{1,0:T(8,128)(2,1)} %all-gather.11.cloned.1.call-done), kind=kOutput, calls=%fused_computation.69 | convolution fusion | flops 2214592512 | bytes 9502720 | tf_op jit(solution)/shard_map/dot_general | solution.py:171
  258.9 85.5 %all-gather.13.cloned.1.call-done = bf16[2048,1408]{1,0:T(8,128)(2,1)} async-done(((bf16[256,1408]{1,0:T(8,128)(2,1)}), bf16[2048,1408]{1,0:T(8,128)(2,1)}) %all-gather.13.cloned.1.call-update) | async-done | bytes 5767184 | tf_op jit(solution)/shard_map/all_gather | solution.py:178
  344.4 93.2 %all-gather.15.cloned.1.call-done = bf16[1408,2048]{1,0:T(8,128)(2,1)} async-done(((bf16[1408,256]{1,0:T(8,128)(2,1)}), bf16[1408,2048]{1,0:T(8,128)(2,1)}) %all-gather.15.cloned.1.call-update) | async-done | bytes 5767184 | tf_op jit(solution)/shard_map/all_gather | solution.py:183
  437.6 0.0 copy-done.8
  437.6 0.0 copy-start.1
  437.6 11.3 %convolution_convert_fusion.2 = bf16[384,2048]{1,0:T(8,128)(2,1)} fusion(bf16[1408,2048]{1,0:T(8,128)(2,1)} %all-gather.15.cloned.1.call-done, bf16[384,2048]{1,0:T(8,128)(2,1)S(1)} %copy-done.8, bf16[2048,1408]{1,0:T(8,128)(2,1)} %all-gather.13.cloned.1.call-done, f32[384,1408]{1,0:T(8,128)} %fusion.43), kind=kOutput, calls=%fused_computation.14 | convolution fusion | flops 4433215488 | bytes 16842752 | tf_op jit(solution)/shard_map/dot_general | solution.py:182
  448.9 0.0 reduce-scatter.2.cloned.1.call-update
  448.9 26.4 %reduce-scatter.2.cloned.1.call-done = bf16[96,2048]{1,0:T(8,128)(2,1)} async-done(((bf16[384,2048]{1,0:T(8,128)(2,1)}), bf16[96,2048]{1,0:T(8,128)(2,1)}) %reduce-scatter.2.cloned.1.call-update) | async-done | bytes 393232 | tf_op jit(solution)/shard_map/reduce_scatter | solution.py:185
  475.3 1.4 fusion.25
  476.7 1.4 multiply_reduce_fusion
  478.2 0.0 copy-done.6
  478.2 2.2 multiply_convert_fusion
  480.4 0.0 copy-done.1
  (13 shorter events, 0.1 us)
Async XLA Ops:
  6.5 65.9 %copy-start = (bf16[512,768]{1,0:T(8,128)(2,1)S(1)}, bf16[512,768]{1,0:T(8,128)(2,1)}, u32[]{:S(2)}) copy-start(bf16[512,768]{1,0:T(8,128)(2,1)} %param.23) | copy-start | bytes 2359300
  6.5 67.7 %copy-start.7 = (s32[384]{0:T(512)S(1)}, s32[384]{0:T(512)}, u32[]{:S(2)}) copy-start(s32[384]{0:T(512)} %param.20) | copy-start | bytes 4612
  6.5 76.5 %all-gather.7.cloned.1.call-start = ((), (), s32[]{:S(2)}) async-start(), calls=%async_computation.2 | async-start | bytes 1769472 | tf_op jit(solution)/shard_map/all_gather | solution.py:152
  74.9 8.1 %copy-start.3 = (bf16[256,512]{1,0:T(8,128)(2,1)S(1)}, bf16[256,512]{1,0:T(8,128)(2,1)}, u32[]{:S(2)}) copy-start(bf16[256,512]{1,0:T(8,128)(2,1)} %param.24) | copy-start | bytes 786436
  98.2 9.1 %copy-start.2 = (bf16[3072,256]{1,0:T(8,128)(2,1)S(1)}, bf16[3072,256]{1,0:T(8,128)(2,1)}, u32[]{:S(2)}) copy-start(bf16[3072,256]{1,0:T(8,128)(2,1)} %all-gather.7.cloned.1.call-done) | copy-start | bytes 4718596
  98.2 9.1 %copy-start.4 = (bf16[256,512]{1,0:T(8,128)(2,1)S(1)}, bf16[256,512]{1,0:T(8,128)(2,1)}, u32[]{:S(2)}) copy-start(bf16[256,512]{1,0:T(8,128)(2,1)} %param.25) | copy-start | bytes 786436
  122.0 10.8 %all-to-all-start = ((bf16[4,96,512]{2,1,0:T(8,128)(2,1)}), bf16[4,96,512]{2,1,0:T(8,128)(2,1)S(1)}, u32[]{:S(2)}, u32[]{:S(2)}) async-start(bf16[4,96,512]{2,1,0:T(8,128)(2,1)} %all_to_all.14), calls=%async_computation | async-start | bytes 786432 | tf_op jit(solution)/shard_map/all_to_all | solution.py:164
  125.4 31.8 %all-gather.9.cloned.1.call-start = ((), (), s32[]{:S(2)}) async-start(), calls=%async_computation.3 | async-start | bytes 1966080 | tf_op jit(solution)/shard_map/all_gather | solution.py:170
  132.8 5.3 %copy-start.5 = (f32[2048]{0:T(1024)S(1)}, f32[2048]{0:T(1024)}, u32[]{:S(2)}) copy-start(f32[2048]{0:T(1024)} %param.27) | copy-start | bytes 24580
  139.1 112.8 %all-gather.11.cloned.1.call-start = ((), (), s32[]{:S(2)}) async-start(), calls=%async_computation.4 | async-start | bytes 6488064 | tf_op jit(solution)/shard_map/all_gather | solution.py:173
  139.8 204.6 %all-gather.13.cloned.1.call-start = ((), (), s32[]{:S(2)}) async-start(), calls=%async_computation.5 | async-start | bytes 6488064 | tf_op jit(solution)/shard_map/all_gather | solution.py:178
  140.4 297.2 %all-gather.15.cloned.1.call-start = ((), (), s32[]{:S(2)}) async-start(), calls=%async_computation.6 | async-start | bytes 6488064 | tf_op jit(solution)/shard_map/all_gather | solution.py:183
  141.0 334.4 %reduce-scatter.2.cloned.1.call-start = ((), (), s32[]{:S(2)}) async-start(), calls=%async_computation.7 | async-start | bytes 1966080 | tf_op jit(solution)/shard_map/reduce_scatter | solution.py:185
  157.3 280.3 %copy-start.8 = (bf16[384,2048]{1,0:T(8,128)(2,1)S(1)}, bf16[384,2048]{1,0:T(8,128)(2,1)}, u32[]{:S(2)}) copy-start(bf16[384,2048]{1,0:T(8,128)(2,1)} %all-gather.9.cloned.1.call-done) | copy-start | bytes 4718596
  437.6 42.8 %copy-start.1 = (bf16[512,768]{1,0:T(8,128)(2,1)S(1)}, bf16[512,768]{1,0:T(8,128)(2,1)}, u32[]{:S(2)}) copy-start(bf16[512,768]{1,0:T(8,128)(2,1)} %param.23) | copy-start | bytes 2359300
  448.9 29.3 %copy-start.6 = (f32[2048]{0:T(1024)S(1)}, f32[2048]{0:T(1024)}, u32[]{:S(2)}) copy-start(f32[2048]{0:T(1024)} %param.31) | copy-start | bytes 24580
Sparse Core Ops, SparseCore 0:
  9.6 49.9 all-gather.6
  139.2 18.0 all-gather.8
  159.5 92.3 all-gather.10
  253.8 90.4 all-gather.12
  346.3 91.2 all-gather.14
  449.1 26.2 reduce-scatter.1
where the time goes:
time: 488 us; the launch traced here: 487 us
  waiting for transfers between devices  325 us (67%)
  matrix products  61.8 us (13%)
  blocking collectives  60 us (12%)
  other arithmetic  21.1 us (4%)
  between operations  13.7 us (3%)
    all_gather x1, waiting for transfers between devices, body(): lax.all_gather(w_gate, 'sp', axis=0, tiled=True)  94.5 us
    all_gather x1, waiting for transfers between devices, body(): lax.all_gather(w_down, 'sp', axis=1, tiled=True)  93.2 us
    all_gather x1, waiting for transfers between devices, body(): lax.all_gather(w_up, 'sp', axis=0, tiled=True)  85.5 us
    all_gather x1, blocking collectives, body(): lax.all_gather(key_rot, 'sp', axis=0, tiled=True)  32.1 us
    all_gather x1, blocking collectives, body(): lax.all_gather(doc_ids, 'sp', axis=0, tiled=True)  27.9 us
    reduce_scatter x1, waiting for transfers between devices, body(): lax.psum_scatter(down_term.astype(jnp.bfloat16), 'tp', scatter_dimension=...  26.4 us
    all_gather x1, waiting for transfers between devices, body(): normed_rows = lax.all_gather(own_normed, 'tp', axis=0, tiled=True)  16.3 us
    dot_general x1, matrix products, attend_rows(): jnp.einsum('qhd,khd->hqk', query_nope, keys_heads, preferred_element_type...  12.7 us
  transfers between devices with their start and end apart: 7, of which 6 were waited for; matrix products, arithmetic and copies ran while one was open for 4% of the time, Pallas kernels for 0%

commit v1 on v0

v1 whole, which is shorter than its diff:
```python
import functools

import jax
import jax.numpy as jnp
from jax import lax
from jax.experimental import pallas as pl
from jax.experimental.pallas import tpu as pltpu
from jax.sharding import PartitionSpec as P

NOPE = 128
RD = 64
VD = 128
QW = 256
CORES = 2

eps_norm = 1e-05
rope_theta = 10000.0
resid_alpha = 8.0**0.25
LOG2E = 1.4426950408889634
NT = (((1,), (1,)), ((), ()))


def rope_angles(positions):
    frequency = rope_theta ** (-jnp.arange(0, RD, 2, dtype=jnp.float32) / RD)
    angles = positions.astype(jnp.float32)[:, None] * frequency[None, :]
    return (jnp.cos(angles), jnp.sin(angles))


def rotate(values, cos_table, sin_table):
    half_width = values.shape[-1] // 2
    first_half = values[..., :half_width]
    second_half = values[..., half_width:]
    return jnp.concatenate(
        [
            first_half * cos_table - second_half * sin_table,
            second_half * cos_table + first_half * sin_table,
        ],
        axis=-1,
    )


def rms_scaled(latent, scaling):
    widened = latent.astype(jnp.float32)
    inverse = lax.rsqrt(jnp.mean(widened * widened, axis=-1, keepdims=True) + eps_norm)
    return (widened * inverse * scaling).astype(jnp.bfloat16)


def layer_scaled(stream, scaling):
    centre = stream - jnp.mean(stream, axis=-1, keepdims=True)
    spread = jnp.mean(centre * centre, axis=-1, keepdims=True)
    return centre * lax.rsqrt(spread + eps_norm) * scaling


def attend_kernel(q_ref, lat_ref, rot_ref, qdoc_ref, kdoc_ref, wk_ref, wv_ref, out_ref, kcat, vals, *, tile):
    @pl.when(pl.program_id(0) == 0)
    def _():
        kcat[:, NOPE:] = rot_ref[...]

    lat = lat_ref[...]
    kcat[:, :NOPE] = jnp.dot(lat, wk_ref[...], preferred_element_type=jnp.float32).astype(jnp.bfloat16)
    vals[...] = jnp.dot(lat, wv_ref[...], preferred_element_type=jnp.float32).astype(jnp.bfloat16)
    factor = (NOPE + RD) ** (-0.5) * LOG2E
    for row in range(0, q_ref.shape[1], tile):
        rows = slice(row, row + tile)
        scores = lax.dot_general(q_ref[0, rows, :], kcat[...], NT, preferred_element_type=jnp.float32)
        scores = jnp.where(qdoc_ref[rows, :] == kdoc_ref[...], scores, -1e30)
        top = jnp.max(scores, axis=-1, keepdims=True)
        weights = jnp.exp2((scores - top) * factor)
        total = jnp.sum(weights, axis=-1, keepdims=True)
        mixed = jnp.dot(weights.astype(jnp.bfloat16), vals[...], preferred_element_type=jnp.float32)
        out_ref[rows, :] = (mixed / total).astype(jnp.bfloat16)


def attend(q, lat, rot, qdoc, kdoc, w_key, w_value):
    heads, rows, _ = q.shape
    keys, width = lat.shape
    tile = 128 if rows % 128 == 0 else rows
    return pl.pallas_call(
        functools.partial(attend_kernel, tile=tile),
        grid=(heads,),
        in_specs=[
            pl.BlockSpec((1, rows, QW), lambda i: (i, 0, 0)),
            pl.BlockSpec((keys, width), lambda i: (0, 0)),
            pl.BlockSpec((keys, QW - NOPE), lambda i: (0, 0)),
            pl.BlockSpec((rows, 1), lambda i: (0, 0)),
            pl.BlockSpec((1, keys), lambda i: (0, 0)),
            pl.BlockSpec((width, NOPE), lambda i: (0, i)),
            pl.BlockSpec((width, VD), lambda i: (0, i)),
        ],
        out_specs=pl.BlockSpec((rows, VD), lambda i: (0, i)),
        out_shape=jax.ShapeDtypeStruct((rows, heads * VD), jnp.bfloat16),
        scratch_shapes=[pltpu.VMEM((keys, QW), jnp.bfloat16), pltpu.VMEM((keys, VD), jnp.bfloat16)],
        compiler_params=pltpu.CompilerParams(vmem_limit_bytes=60 * 1024 * 1024),
        cost_estimate=pl.CostEstimate(
            flops=2 * heads * keys * (rows * (QW + VD) + width * (NOPE + VD)),
            bytes_accessed=2 * (heads * rows * QW + keys * (width + QW)),
            transcendentals=heads * rows * keys,
        ),
        name="attend",
    )(q, lat, rot, qdoc, kdoc, w_key, w_value)


def hidden_kernel(index_ref, xa_ref, xb_ref, *rest, n_pieces, tile):
    pieces = rest[:n_pieces]
    out_ref, gate_w, up_w, sems = rest[n_pieces:]
    units, width = pieces[0].shape
    units //= 2
    copies = []
    for i, piece in enumerate(pieces):
        place = pl.ds(pl.multiple_of(index_ref[i] * width, width), width)
        copies.append(pltpu.make_async_copy(piece.at[pl.ds(0, units)], gate_w.at[:, place], sems.at[2 * i]))
        copies.append(pltpu.make_async_copy(piece.at[pl.ds(units, units)], up_w.at[:, place], sems.at[2 * i + 1]))
    for copy in copies:
        copy.start()
    for copy in copies:
        copy.wait()
    half = xa_ref.shape[0]
    for base, x_ref in ((0, xa_ref), (half, xb_ref)):
        for row in range(0, half, tile):
            x = x_ref[row : row + tile, :]
            gate = lax.dot_general(x, gate_w[...], NT, preferred_element_type=jnp.float32)
            up = lax.dot_general(x, up_w[...], NT, preferred_element_type=jnp.float32)
            out_ref[base + row : base + row + tile, :] = (gate / (1.0 + jnp.exp(-gate)) * up).astype(jnp.bfloat16)


def hidden_units(index, xa, xb, pieces):
    units = pieces[0].shape[0] // 2
    half, width = xa.shape
    tile = 128 if half % 128 == 0 else half
    n = len(pieces)
    vmem = pl.BlockSpec(memory_space=pltpu.VMEM)
    return pl.pallas_call(
        functools.partial(hidden_kernel, n_pieces=n, tile=tile),
        in_specs=[pl.BlockSpec(memory_space=pltpu.SMEM), vmem, vmem] + [pl.BlockSpec(memory_space=pl.ANY)] * n,
        out_specs=vmem,
        out_shape=jax.ShapeDtypeStruct((2 * half, units), jnp.bfloat16),
        scratch_shapes=[
            pltpu.VMEM((units, width), jnp.bfloat16),
            pltpu.VMEM((units, width), jnp.bfloat16),
            pltpu.SemaphoreType.DMA((2 * n,)),
        ],
        compiler_params=pltpu.CompilerParams(vmem_limit_bytes=60 * 1024 * 1024),
        cost_estimate=pl.CostEstimate(
            flops=8 * half * units * width, bytes_accessed=4 * units * width + 4 * half * width, transcendentals=2 * half * units
        ),
        name="hidden_units",
    )(index, xa, xb, *pieces)


def body(
    resid_stream,
    q_latent,
    kv_latent,
    rope_key,
    doc_ids,
    q_gain,
    kv_gain,
    w_query,
    w_key,
    w_value,
    w_out,
    mix_gain,
    w_gate,
    w_up,
    w_down,
    out_gain,
):
    bf16 = jnp.bfloat16
    f32 = jnp.float32
    tok_rows = q_latent.shape[0]
    heads = w_key.shape[1] // NOPE
    n_sp = lax.axis_size("sp")
    n_tp = lax.axis_size("tp")
    n_x = n_tp // CORES
    n_y = n_x if n_sp % (2 * n_x) == 0 else 1
    n_h = 2
    n_l = n_sp // (n_h * n_y)
    sp = lax.axis_index("sp")
    tp = lax.axis_index("tp")
    at_y = sp % n_y
    at_l = (sp // n_y) % n_l
    at_h = sp // (n_y * n_l)
    at_core = tp % CORES
    d_block = w_gate.shape[0]
    ff_block = w_gate.shape[1]
    units = ff_block // n_l
    part_rows = tok_rows // n_tp
    half_rows = tok_rows // CORES

    def sp_move(value, dh, dl, dy):
        pairs = []
        for s in range(n_sp):
            y, l, h = s % n_y, (s // n_y) % n_l, s // (n_y * n_l)
            pairs.append((s, (((h + dh) % n_h) * n_l + (l + dl) % n_l) * n_y + (y + dy) % n_y))
        return lax.ppermute(value, "sp", pairs)

    def lx_move(value, dl, dx):
        pairs = []
        for s in range(n_sp):
            y, l, h = s % n_y, (s // n_y) % n_l, s // (n_y * n_l)
            to_sp = (h * n_l + (l + dl) % n_l) * n_y + y
            for t in range(n_tp):
                x, core = t // CORES, t % CORES
                pairs.append((s * n_tp + t, to_sp * n_tp + ((x + dx) % n_x) * CORES + core))
        return lax.ppermute(value, ("sp", "tp"), pairs)

    def core_swap(value):
        return lax.ppermute(value, "tp", [(t, t // CORES * CORES + (t + 1) % CORES) for t in range(n_tp)])

    z_steps = [(dh, dl) for dh in range(n_h) for dl in range(n_l)]

    positions = sp * tok_rows + jnp.arange(tok_rows, dtype=jnp.int32)
    cos_table, sin_table = rope_angles(positions)
    kv_normed = rms_scaled(kv_latent, kv_gain)
    key_rot = rotate(rope_key.astype(f32), cos_table, sin_table).astype(bf16)
    doc_code = jnp.stack([doc_ids // 128, doc_ids % 128], axis=1).astype(bf16)
    packed = jnp.concatenate([kv_normed, key_rot, doc_code], axis=1)
    packed = lax.dynamic_slice_in_dim(packed, at_core * half_rows, half_rows, 0)
    packs = [packed if (dh, dl) == (0, 0) else sp_move(packed, dh, dl, 0) for dh, dl in z_steps]
    packs = packs + [sp_move(p, 0, 0, dy) for p in packs for dy in range(1, n_y)]
    pack_half = jnp.concatenate(packs, axis=0)
    pack_all = jnp.concatenate([pack_half, core_swap(pack_half)], axis=0)
    key_width = kv_latent.shape[1]
    lat = pack_all[:, :key_width]
    rot = jnp.pad(pack_all[:, key_width : key_width + RD], ((0, 0), (0, QW - NOPE - RD)))
    codes = pack_all[:, key_width + RD :].astype(jnp.int32)
    kdoc = (codes[:, 0] * 128 + codes[:, 1])[None, :]

    def halves(weight):
        mine = lax.dynamic_slice_in_dim(weight, at_l * units, units, 0)
        return [mine] + [
            lax.dynamic_slice_in_dim(weight, ((at_l + dl) % n_l) * units, units, 0) for dl in range(1, n_l)
        ]

    gate_halves = halves(w_gate.T)
    up_halves = halves(w_up.T)
    gate_up = [jnp.concatenate([g, u], axis=0) for g, u in zip(gate_halves, up_halves)]
    down = halves(w_down)

    def spread(parts):
        over_z = [parts[dl] if (dh, dl) == (0, 0) else sp_move(parts[dl], dh, dl, 0) for dh, dl in z_steps]
        return {
            (dh, dl, dy): over_z[i] if dy == 0 else sp_move(over_z[i], 0, 0, dy)
            for i, (dh, dl) in enumerate(z_steps)
            for dy in range(n_y)
        }

    gate_up_pieces = spread(gate_up)
    down_pieces = spread(down)

    def block_of(dh, dl, dy):
        return (((at_h - dh) % n_h) * n_l + (at_l - dl) % n_l) * n_y + (at_y - dy) % n_y

    q_normed = rms_scaled(q_latent, q_gain)
    queries = jnp.dot(q_normed, w_query, preferred_element_type=f32).reshape(tok_rows, heads, NOPE + RD)
    turned = rotate(queries[:, :, NOPE:], cos_table[:, None, :], sin_table[:, None, :])
    q_rows = jnp.concatenate(
        [queries[:, :, :NOPE], turned, jnp.zeros((tok_rows, heads, QW - NOPE - RD), f32)], axis=-1
    ).astype(bf16)
    attended = attend(jnp.transpose(q_rows, (1, 0, 2)), lat, rot, doc_ids[:, None], kdoc, w_key, w_value)

    heads_rows = lax.all_to_all(attended, "tp", split_axis=0, concat_axis=1, tiled=True)
    mixer_out = jnp.dot(heads_rows, w_out, preferred_element_type=f32)
    own_resid = lax.dynamic_slice_in_dim(resid_stream, tp * part_rows, part_rows, 0)
    own_normed = layer_scaled(resid_alpha * own_resid.astype(f32) + mixer_out, mix_gain).astype(bf16)

    lx_steps = [(dl, dx) for dl in range(n_l) for dx in range(n_x)]
    rows_a = jnp.concatenate(
        [own_normed if step == (0, 0) else lx_move(own_normed, *step) for step in lx_steps], axis=0
    )
    rows_b = core_swap(rows_a)
    keys = [(dh, dl, dy) for dh, dl in z_steps for dy in range(n_y)]
    if d_block % 128 == 0:
        index = jnp.stack([block_of(*k) for k in keys]).astype(jnp.int32)
        hidden = hidden_units(index, rows_a, rows_b, [gate_up_pieces[k] for k in keys])
    else:
        gathered = jnp.zeros((n_sp, 2 * units, d_block), bf16)
        for k in keys:
            gathered = lax.dynamic_update_slice_in_dim(gathered, gate_up_pieces[k][None], block_of(*k), 0)
        weight = jnp.transpose(gathered, (1, 0, 2)).reshape(2 * units, n_sp * d_block)
        both = lax.dot_general(jnp.concatenate([rows_a, rows_b]), weight, NT, preferred_element_type=f32)
        hidden = (jax.nn.silu(both[:, :units]) * both[:, units:]).astype(bf16)

    group_rows = rows_a.shape[0]
    sums = {}
    chunks = [[(0, dy) for dy in range(n_y)]] + [[(dh, dy) for dh in range(1, n_h) for dy in range(n_y)]]
    for chunk in chunks:
        parts = []
        for dh, dy in chunk:
            outs = [jnp.dot(hidden, down_pieces[(dh, dl, dy)], preferred_element_type=f32) for dl in range(n_l)]
            stacked = jnp.stack(outs)
            parts.append(jnp.take(stacked, (at_l - jnp.arange(n_l)) % n_l, axis=0))
        partial = jnp.concatenate(parts, axis=0)
        other = core_swap(partial[:, group_rows:].astype(bf16))
        mine = (partial[:, :group_rows] + other.astype(f32)).astype(bf16)
        total = 0.0
        for i, (dl, dx) in enumerate(lx_steps):
            block = mine[:, i * part_rows : (i + 1) * part_rows]
            moved = block if (dl, dx) == (0, 0) else lx_move(block, -dl, -dx)
            total = total + moved.astype(f32)
        for i, pair in enumerate(chunk):
            sums[pair] = total[i * n_l : (i + 1) * n_l]

    pairs = [(dh, dy) for dh in range(n_h) for dy in range(n_y)]
    stacked = jnp.stack([sums[p] for p in pairs]).reshape(n_h, n_y, n_l, part_rows, d_block)
    stacked = jnp.take(stacked, (at_h - jnp.arange(n_h)) % n_h, axis=0)
    stacked = jnp.take(stacked, (at_y - jnp.arange(n_y)) % n_y, axis=1)
    ffn_sum = jnp.transpose(stacked, (3, 0, 2, 1, 4)).reshape(part_rows, n_sp * d_block)
    return layer_scaled(resid_alpha * own_normed.astype(f32) + 0.5 * ffn_sum, out_gain).astype(bf16)


def solution(mesh):
    in_specs = (
        P("sp", None),
        P("sp", None),
        P("sp", None),
        P("sp", None),
        P("sp"),
        P(),
        P(),
        P(None, "tp"),
        P(None, "tp"),
        P(None, "tp"),
        P(),
        P(),
        P("sp", "tp"),
        P("sp", "tp"),
        P("tp", "sp"),
        P(),
    )
    out_specs = P(("sp", "tp"), None)
    return jax.shard_map(body, mesh=mesh, in_specs=in_specs, out_specs=out_specs, check_vma=False)
```

time: 488 us -> 336 us (0.69)
  waiting for transfers between devices: 325 us -> 181 us
  blocking collectives: 60 us -> 0 us
  matrix products: 61.8 us -> 17 us
  starting transfers between devices: 3.88 us -> 39.6 us
  Pallas kernels: 0 us -> 35.3 us
  local copies, waits for them, and re-layouts: 1.9 us -> 36.3 us
  between operations: 13.7 us -> 0.75 us
    all_gather x5 -> x0, waiting for transfers between devices: 289 us -> none  [the longest x1 94.5 us: body(): lax.all_gather(w_gate, 'sp', axis=0, tiled=True)]
    ppermute x0 -> x34, waiting for transfers between devices: none -> 179 us  [the longest x21 142 us: sp_move(): return lax.ppermute(value, 'sp', pairs)]
    all_gather x2 -> x0, blocking collectives: 60 us -> none  [the longest x1 32.1 us: body(): lax.all_gather(key_rot, 'sp', axis=0, tiled=True)]
    dot_general x9 -> x10, matrix products: 61.8 us -> 17 us  [the longest x8 11.3 us: body(): jnp.dot(hidden, down_pieces[dh, dl, dy], preferred_element_type=f32)]
    ppermute x0 -> x34, starting transfers between devices: none -> 36 us  [the longest x21 26.6 us: sp_move(): return lax.ppermute(value, 'sp', pairs)]
    pallas_call x0 -> x2, Pallas kernels: none -> 35.3 us  [the longest x1 19 us: attend(): pl.pallas_call(functools.partial(attend_kernel, tile=tile), grid=(heads,)...]
    reduce_scatter x1 -> x0, waiting for transfers between devices: 26.4 us -> none  [body(): lax.psum_scatter(down_term.astype(jnp.bfloat16), 'tp', scatter_dimension=...]
    gather x0 -> x6, local copies, waits for them, and re-layouts: none -> 14.2 us  [the longest x4 13 us: body(): parts.append(jnp.take(stacked, (at_l - jnp.arange(n_l)) % n_l, axis=0))]
  transfers between devices with their start and end apart: 7 -> 35, of which waited for: 6 -> 18; matrix products, arithmetic and copies ran while one was open for 4% -> 14% of each run, Pallas kernels for 0% -> 5%
where the time goes in v1:
time: 336 us; the launch traced here: 335 us
  waiting for transfers between devices  181 us (54%)
  starting transfers between devices  39.6 us (12%)
  local copies, waits for them, and re-layouts  36.3 us (11%)
  Pallas kernels  35.3 us (11%)
  other arithmetic  24.7 us (7%)
  matrix products  17 us (5%)
    ppermute x21, waiting for transfers between devices, sp_move(): return lax.ppermute(value, 'sp', pairs)  142 us
    ppermute x9, waiting for transfers between devices, lx_move(): return lax.ppermute(value, ('sp', 'tp'), pairs)  35.1 us
    ppermute x21, starting transfers between devices, sp_move(): return lax.ppermute(value, 'sp', pairs)  26.6 us
    pallas_call x1, Pallas kernels, attend(): pl.pallas_call(functools.partial(attend_kernel, tile=tile), grid=(heads,)...  19 us
    pallas_call x1, Pallas kernels, hidden_units(): pl.pallas_call(functools.partial(hidden_kernel, n_pieces=n, tile=tile), i...  16.3 us
    gather x4, local copies, waits for them, and re-layouts, body(): parts.append(jnp.take(stacked, (at_l - jnp.arange(n_l)) % n_l, axis=0))  13 us
    dot_general x8, matrix products, body(): jnp.dot(hidden, down_pieces[dh, dl, dy], preferred_element_type=f32)  11.3 us
    ppermute x9, starting transfers between devices, lx_move(): return lax.ppermute(value, ('sp', 'tp'), pairs)  8.7 us
  transfers between devices with their start and end apart: 35, of which 18 were waited for; matrix products, arithmetic and copies ran while one was open for 14% of the time, Pallas kernels for 5%

profile of v1, /device:TPU:0, one launch (start us, length us, event | category | flops | bytes accessed | tf_op | source)
XLA Modules:
  0.0 335.1 jit_solution(15044598725351258045)
XLA Ops:
  2.1 1.1 fusion.12
  4.2 1.6 add_convert_fusion.1
  6.0 3.1 collective-permute-start
  9.2 2.6 collective-permute-start.1
  11.7 1.7 collective-permute-start.3
  15.1 1.6 collective-permute-start.4
  16.8 6.3 %collective-permute-done.1 = bf16[192,322]{1,0:T(8,128)(2,1)S(1)} collective-permute-done((bf16[192,322]{1,0:T(8,128)(2,1)S(1)}, bf16[192,322]{1,0:T(8,128)(2,1)S(1)}, u32[]{:S(2)}, u32[]{:S(2)}) %collective-permute-start.1) | collective-permute-done | bytes 123680 | tf_op jit(solution)/shard_map/ppermute | solution.py:195
  23.1 1.5 collective-permute-start.5
  30.5 1.4 copy.61
  33.6 1.2 subtract_convert_fusion
  34.8 1.2 maximum_bitcast_fusion.q_ref
  36.8 1.2 constant_dynamic-update-slice_fusion.8
  37.9 1.5 slice_convert_fusion
  39.4 1.2 slice.128
  40.6 2.7 slice.127.lat_ref
  43.3 1.5 fusion.8
  45.9 19.0 %attend.1 = bf16[384,512]{1,0:T(8,128)(2,1)} custom-call(bf16[4,384,256]{2,1,0:T(8,128)(2,1)} %maximum_bitcast_fusion.q_ref, bf16[3072,256]{1,0:T(8,128)(2,1)} %slice.127.lat_ref, bf16[3072,128]{1,0:T(8,128)(2,1)} %pad.4.rot_ref, s32[384,1]{1,0:T(8,128)} %broadcast_in_dim.70.qdoc_ref, s32[1,3072]{1,0:T(1,128)} %bitcast.80, bf16[256,512]{1,0:T(8,128)(2,1)} %wk_ref.1, ...), custom_call_target="tpu_custom_call" | custom-call | flops 5234491392 | bytes 3932160 | tf_op jit(solution)/shard_map/attend/pallas_call | solution.py:78
  64.9 3.6 %all-to-all-start = ((bf16[4,96,512]{2,1,0:T(8,128)(2,1)}), bf16[4,96,512]{2,1,0:T(8,128)(2,1)S(1)}, u32[]{:S(2)}, u32[]{:S(2)}) async-start(bf16[4,96,512]{2,1,0:T(8,128)(2,1)} %bitcast.79), calls=%async_computation | async-start | bytes 786432 | tf_op jit(solution)/shard_map/all_to_all | solution.py:262
  69.5 1.3 collective-permute-start.19
  70.8 2.5 collective-permute-start.27
  73.3 2.4 all-to-all-done
  75.8 5.0 %fusion.33 = (f32[96]{0:T(128)S(1)}, f32[96,2048]{1,0:T(8,128)S(1)}) fusion(bf16[96,2048]{1,0:T(8,128)(2,1)S(1)} %bitcast.73, bf16[2048,2048]{1,0:T(8,128)(2,1)} %param.28, bf16[384,2048]{1,0:T(8,128)(2,1)} %param.18, s32[]{:T(128)S(6)} %select_n.206), kind=kOutput, calls=%fused_computation.158 | convolution fusion | flops 806092672 | bytes 9961860 | tf_op jit(solution)/shard_map/dot_general | solution.py:263
  81.2 1.2 collective-permute-start.10
  82.5 1.6 collective-permute-start.8
  87.0 12.6 %collective-permute-done.10 = bf16[96,2048]{1,0:T(8,128)(2,1)} collective-permute-done((bf16[96,2048]{1,0:T(8,128)(2,1)S(1)}, bf16[96,2048]{1,0:T(8,128)(2,1)}, u32[]{:S(2)}, u32[]{:S(2)}) %collective-permute-start.10) | collective-permute-done | bytes 393248 | tf_op jit(solution)/shard_map/ppermute | solution.py:205
  99.9 1.8 collective-permute-done.8
  101.7 5.4 %collective-permute-done.9 = bf16[96,2048]{1,0:T(8,128)(2,1)} collective-permute-done((bf16[96,2048]{1,0:T(8,128)(2,1)S(1)}, bf16[96,2048]{1,0:T(8,128)(2,1)}, u32[]{:S(2)}, u32[]{:S(2)}) %collective-permute-start.9) | collective-permute-done | bytes 393248 | tf_op jit(solution)/shard_map/ppermute | solution.py:205
  107.1 1.3 pad_maximum_fusion.2.xa_ref
  110.5 1.4 collective-permute-start.17
  112.0 1.1 collective-permute-start.26
  113.1 78.0 %collective-permute-done.26 = bf16[704,256]{1,0:T(8,128)(2,1)} collective-permute-done((bf16[704,256]{1,0:T(8,128)(2,1)}, bf16[704,256]{1,0:T(8,128)(2,1)}, u32[]{:S(2)}, u32[]{:S(2)}) %collective-permute-start.26) | collective-permute-done | bytes 360480 | tf_op jit(solution)/shard_map/ppermute | solution.py:195
  192.0 1.1 collective-permute-start.14
  194.1 1.1 collective-permute-start.18
  196.3 14.1 %collective-permute-done.12.rest_1_ = bf16[1408,256]{1,0:T(8,128)(2,1)} collective-permute-done((bf16[1408,256]{1,0:T(8,128)(2,1)}, bf16[1408,256]{1,0:T(8,128)(2,1)}, u32[]{:S(2)}, u32[]{:S(2)}) %collective-permute-start.12) | collective-permute-done | bytes 720928 | tf_op jit(solution)/shard_map/ppermute | solution.py:195
  211.3 14.5 %collective-permute-done.14.rest_3_ = bf16[1408,256]{1,0:T(8,128)(2,1)} collective-permute-done((bf16[1408,256]{1,0:T(8,128)(2,1)}, bf16[1408,256]{1,0:T(8,128)(2,1)}, u32[]{:S(2)}, u32[]{:S(2)}) %collective-permute-start.14) | collective-permute-done | bytes 720928 | tf_op jit(solution)/shard_map/ppermute | solution.py:195
  226.8 14.5 %collective-permute-done.16.rest_5_ = bf16[1408,256]{1,0:T(8,128)(2,1)} collective-permute-done((bf16[1408,256]{1,0:T(8,128)(2,1)S(1)}, bf16[1408,256]{1,0:T(8,128)(2,1)}, u32[]{:S(2)}, u32[]{:S(2)}) %collective-permute-start.16) | collective-permute-done | bytes 720928 | tf_op jit(solution)/shard_map/ppermute | solution.py:195
  242.2 14.5 %collective-permute-done.18.rest_7_ = bf16[1408,256]{1,0:T(8,128)(2,1)} collective-permute-done((bf16[1408,256]{1,0:T(8,128)(2,1)}, bf16[1408,256]{1,0:T(8,128)(2,1)}, u32[]{:S(2)}, u32[]{:S(2)}) %collective-permute-start.18) | collective-permute-done | bytes 720928 | tf_op jit(solution)/shard_map/ppermute | solution.py:195
  257.7 16.3 %hidden_units.1 = bf16[768,704]{1,0:T(8,128)(2,1)} custom-call(s32[8]{0:T(128)} %stack.98.index_ref, bf16[384,2048]{1,0:T(8,128)(2,1)} %copy-done.4, bf16[384,2048]{1,0:T(8,128)(2,1)} %collective-permute-done.11.xb_ref, bf16[1408,256]{1,0:T(8,128)(2,1)} %pad_maximum_fusion.8.rest_0_, bf16[1408,256]{1,0:T(8,128)(2,1)} %collective-permute-done.12.rest_1_, ...), custom_call_target="tpu_custom_call" | custom-call | flops 4429185024 | bytes 8912896 | tf_op jit(solution)/shard_map/hidden_units/pallas_call | solution.py:132
  274.0 2.1 convolution_bitcast_fusion.7
  276.1 1.5 convolution_bitcast_fusion.6
  277.6 1.5 convolution_bitcast_fusion.2
  279.0 1.5 convolution_bitcast_fusion.3
  281.0 1.5 convolution_bitcast_fusion.1
  282.5 1.2 pad_maximum_fusion.3
  283.7 1.3 pad_maximum_fusion.6
  285.0 3.2 gather_fusion.2
  288.2 3.2 gather_fusion.5
  291.4 1.3 pad_maximum_fusion.5
  292.7 3.2 gather_fusion.4
  295.9 1.5 convolution_bitcast_fusion.5
  297.4 1.5 convolution_bitcast_fusion.4
  298.9 1.3 pad_maximum_fusion.4
  300.2 3.3 gather_fusion.3
  303.5 3.0 broadcast_select_fusion.2
  307.4 1.6 collective-permute-done.22
  309.3 1.6 collective-permute-start.23
  310.9 2.0 collective-permute-start.25
  313.2 1.6 collective-permute-start.31
  314.8 3.1 collective-permute-done.23
  318.7 4.2 %collective-permute-done.25 = bf16[4,96,256]{2,1,0:T(8,128)(2,1)S(1)} collective-permute-done((bf16[4,96,256]{2,1,0:T(8,128)(2,1)S(1)}, bf16[4,96,256]{2,1,0:T(8,128)(2,1)S(1)}, u32[]{:S(2)}, u32[]{:S(2)}) %collective-permute-start.25) | collective-permute-done | bytes 196640 | tf_op jit(solution)/shard_map/ppermute | solution.py:205
  323.0 1.7 collective-permute-done.31
  324.8 2.4 collective-permute-done.32
  327.2 3.0 collective-permute-done.33
  333.9 1.1 multiply_convert_fusion
  (150 shorter events, 34.3 us)
Async XLA Ops:
  0.0 31.9 %copy-start = (bf16[512,768]{1,0:T(8,128)(2,1)S(1)}, bf16[512,768]{1,0:T(8,128)(2,1)}, u32[]{:S(2)}) copy-start(bf16[512,768]{1,0:T(8,128)(2,1)} %param.25) | copy-start | bytes 2359300
  1.1 12.4 %copy-start.5 = (bf16[384,512]{1,0:T(8,128)(2,1)S(1)}, bf16[384,512]{1,0:T(8,128)(2,1)}, u32[]{:S(2)}) copy-start(bf16[384,512]{1,0:T(8,128)(2,1)} %param.19) | copy-start | bytes 1179652
  3.1 10.5 %copy-start.14 = (s32[384]{0:T(512)S(1)}, s32[384]{0:T(512)}, u32[]{:S(2)}) copy-start(s32[384]{0:T(512)} %param.22) | copy-start | bytes 4612
  6.0 9.1 %collective-permute-start = (bf16[192,322]{1,0:T(8,128)(2,1)S(1)}, bf16[192,322]{1,0:T(8,128)(2,1)S(1)}, u32[]{:S(2)}, u32[]{:S(2)}) collective-permute-start(bf16[192,322]{1,0:T(8,128)(2,1)S(1)} %get-tuple-element.7), channel_id=1, source_target_pairs={{0,8},{4,12},{8,0},{12,4},{16,24},{20,28},{24,16},{28,20},{1,9},{5... | collective-permute-start | bytes 370952 | tf_op jit(solution)/shard_map/ppermute | solution.py:195
  9.2 13.9 %collective-permute-start.1 = (bf16[192,322]{1,0:T(8,128)(2,1)S(1)}, bf16[192,322]{1,0:T(8,128)(2,1)S(1)}, u32[]{:S(2)}, u32[]{:S(2)}) collective-permute-start(bf16[192,322]{1,0:T(8,128)(2,1)S(1)} %get-tuple-element.7), channel_id=1, source_target_pairs={{0,16},{4,20},{8,24},{12,28},{16,0},{20,4},{24,8},{28,12},{1,17},{... | collective-permute-start | bytes 370952 | tf_op jit(solution)/shard_map/ppermute | solution.py:195
  11.7 12.9 %collective-permute-start.2 = (bf16[192,322]{1,0:T(8,128)(2,1)S(1)}, bf16[192,322]{1,0:T(8,128)(2,1)S(1)}, u32[]{:S(2)}, u32[]{:S(2)}) collective-permute-start(bf16[192,322]{1,0:T(8,128)(2,1)S(1)} %get-tuple-element.7), channel_id=1, source_target_pairs={{0,24},{4,28},{8,16},{12,20},{16,8},{20,12},{24,0},{28,4},{1,25},{... | collective-permute-start | bytes 370952 | tf_op jit(solution)/shard_map/ppermute | solution.py:195
  11.7 15.5 %collective-permute-start.3 = (bf16[192,322]{1,0:T(8,128)(2,1)S(1)}, bf16[192,322]{1,0:T(8,128)(2,1)S(1)}, u32[]{:S(2)}, u32[]{:S(2)}) collective-permute-start(bf16[192,322]{1,0:T(8,128)(2,1)S(1)} %get-tuple-element.7), channel_id=1, source_target_pairs={{0,4},{4,0},{8,12},{12,8},{16,20},{20,16},{24,28},{28,24},{1,5},{5... | collective-permute-start | bytes 370952 | tf_op jit(solution)/shard_map/ppermute | solution.py:195
  15.1 12.8 %collective-permute-start.4 = (bf16[192,322]{1,0:T(8,128)(2,1)S(1)}, bf16[192,322]{1,0:T(8,128)(2,1)S(1)}, u32[]{:S(2)}, u32[]{:S(2)}) collective-permute-start(bf16[192,322]{1,0:T(8,128)(2,1)S(1)} %collective-permute-done), channel_id=1, source_target_pairs={{0,4},{4,0},{8,12},{12,8},{16,20},{20,16},{24,28},{28,24},{1,5},{5... | collective-permute-start | bytes 370952 | tf_op jit(solution)/shard_map/ppermute | solution.py:195
  23.1 5.5 %collective-permute-start.5 = (bf16[192,322]{1,0:T(8,128)(2,1)S(1)}, bf16[192,322]{1,0:T(8,128)(2,1)S(1)}, u32[]{:S(2)}, u32[]{:S(2)}) collective-permute-start(bf16[192,322]{1,0:T(8,128)(2,1)S(1)} %collective-permute-done.1), channel_id=1, source_target_pairs={{0,4},{4,0},{8,12},{12,8},{16,20},{20,16},{24,28},{28,24},{1,5},{5... | collective-permute-start | bytes 370952 | tf_op jit(solution)/shard_map/ppermute | solution.py:195
  24.6 5.2 %collective-permute-start.6 = (bf16[192,322]{1,0:T(8,128)(2,1)S(1)}, bf16[192,322]{1,0:T(8,128)(2,1)S(1)}, u32[]{:S(2)}, u32[]{:S(2)}) collective-permute-start(bf16[192,322]{1,0:T(8,128)(2,1)S(1)} %collective-permute-done.2), channel_id=1, source_target_pairs={{0,4},{4,0},{8,12},{12,8},{16,20},{20,16},{24,28},{28,24},{1,5},{5... | collective-permute-start | bytes 370952 | tf_op jit(solution)/shard_map/ppermute | solution.py:195
  28.6 3.3 copy-start.15
  31.9 4.1 %collective-permute-start.7 = (bf16[1536,322]{0,1:T(8,128)(2,1)}, bf16[1536,322]{0,1:T(8,128)(2,1)S(1)}, u32[]{:S(2)}, u32[]{:S(2)}) collective-permute-start(bf16[1536,322]{0,1:T(8,128)(2,1)} %copy.61), channel_id=1, source_target_pairs={{0,1},{1,0},{2,3},{3,2},{4,5},{5,4},{6,7},{7,6},{8,9},{9,8},{10,11... | collective-permute-start | bytes 2967560 | tf_op jit(solution)/shard_map/ppermute | solution.py:208
  45.9 22.7 %copy-start.9 = (bf16[1408,256]{1,0:T(8,128)(2,1)S(1)}, bf16[1408,256]{1,0:T(8,128)(2,1)}, u32[]{:S(2)}) copy-start(bf16[1408,256]{1,0:T(8,128)(2,1)} %param.32) | copy-start | bytes 2162692
  64.9 10.8 %all-to-all-start = ((bf16[4,96,512]{2,1,0:T(8,128)(2,1)}), bf16[4,96,512]{2,1,0:T(8,128)(2,1)S(1)}, u32[]{:S(2)}, u32[]{:S(2)}) async-start(bf16[4,96,512]{2,1,0:T(8,128)(2,1)} %bitcast.79), calls=%async_computation | async-start | bytes 786432 | tf_op jit(solution)/shard_map/all_to_all | solution.py:262
  69.5 41.0 %collective-permute-start.19 = (bf16[704,256]{1,0:T(8,128)(2,1)}, bf16[704,256]{1,0:T(8,128)(2,1)}, u32[]{:S(2)}, u32[]{:S(2)}) collective-permute-start(bf16[704,256]{1,0:T(8,128)(2,1)} %get-tuple-element.19), channel_id=1, source_target_pairs={{0,8},{4,12},{8,0},{12,4},{16,24},{20,28},{24,16},{28,20},{1,9},{5... | collective-permute-start | bytes 1081352 | tf_op jit(solution)/shard_map/ppermute | solution.py:195
  70.8 41.1 %collective-permute-start.27 = (bf16[704,256]{1,0:T(8,128)(2,1)}, bf16[704,256]{1,0:T(8,128)(2,1)}, u32[]{:S(2)}, u32[]{:S(2)}) collective-permute-start(bf16[704,256]{1,0:T(8,128)(2,1)} %get-tuple-element.19), channel_id=1, source_target_pairs={{0,24},{4,28},{8,16},{12,20},{16,8},{20,12},{24,0},{28,4},{1,25},{... | collective-permute-start | bytes 1081352 | tf_op jit(solution)/shard_map/ppermute | solution.py:195
  75.7 5.3 %copy-start.10 = (f32[2048]{0:T(1024)S(1)}, f32[2048]{0:T(1024)}, u32[]{:S(2)}) copy-start(f32[2048]{0:T(1024)} %param.29) | copy-start | bytes 24580
  80.7 4.0 %copy-start.7 = (bf16[256,1408]{1,0:T(8,128)(2,1)S(1)}, bf16[256,1408]{1,0:T(8,128)(2,1)}, u32[]{:S(2)}) copy-start(bf16[256,1408]{1,0:T(8,128)(2,1)} %param.31) | copy-start | bytes 2162692
  80.7 4.0 %copy-start.8 = (bf16[256,1408]{1,0:T(8,128)(2,1)S(1)}, bf16[256,1408]{1,0:T(8,128)(2,1)}, u32[]{:S(2)}) copy-start(bf16[256,1408]{1,0:T(8,128)(2,1)} %param.30) | copy-start | bytes 2162692
  81.0 3.0 copy-start.11
  81.2 18.4 %collective-permute-start.10 = (bf16[96,2048]{1,0:T(8,128)(2,1)S(1)}, bf16[96,2048]{1,0:T(8,128)(2,1)}, u32[]{:S(2)}, u32[]{:S(2)}) collective-permute-start(bf16[96,2048]{1,0:T(8,128)(2,1)S(1)} %multiply_convert_fusion.1), channel_id=1, source_target_pairs={{0,10},{1,11},{2,8},{3,9},{4,14},{5,15},{6,12},{7,13},{8,2},{9,3},... | collective-permute-start | bytes 1179656 | tf_op jit(solution)/shard_map/ppermute | solution.py:205
  82.5 19.3 %collective-permute-start.8 = (bf16[96,2048]{1,0:T(8,128)(2,1)S(1)}, bf16[96,2048]{1,0:T(8,128)(2,1)}, u32[]{:S(2)}, u32[]{:S(2)}) collective-permute-start(bf16[96,2048]{1,0:T(8,128)(2,1)S(1)} %multiply_convert_fusion.1), channel_id=1, source_target_pairs={{0,2},{1,3},{2,0},{3,1},{4,6},{5,7},{6,4},{7,5},{8,10},{9,11},{10,... | collective-permute-start | bytes 1179656 | tf_op jit(solution)/shard_map/ppermute | solution.py:205
  84.1 23.0 %collective-permute-start.9 = (bf16[96,2048]{1,0:T(8,128)(2,1)S(1)}, bf16[96,2048]{1,0:T(8,128)(2,1)}, u32[]{:S(2)}, u32[]{:S(2)}) collective-permute-start(bf16[96,2048]{1,0:T(8,128)(2,1)S(1)} %multiply_convert_fusion.1), channel_id=1, source_target_pairs={{0,8},{1,9},{2,10},{3,11},{4,12},{5,13},{6,14},{7,15},{8,0},{9,1},... | collective-permute-start | bytes 1179656 | tf_op jit(solution)/shard_map/ppermute | solution.py:205
  87.0 21.5 %copy-start.6 = (bf16[256,704]{0,1:T(8,128)(2,1)S(1)}, bf16[256,704]{0,1:T(8,128)(2,1)}, u32[]{:S(2)}) copy-start(bf16[256,704]{0,1:T(8,128)(2,1)} %copy.75) | copy-start | bytes 1081348
  99.6 92.4 %collective-permute-start.13 = (bf16[1408,256]{1,0:T(8,128)(2,1)S(1)}, bf16[1408,256]{1,0:T(8,128)(2,1)}, u32[]{:S(2)}, u32[]{:S(2)}) collective-permute-start(bf16[1408,256]{1,0:T(8,128)(2,1)S(1)} %pad_maximum_fusion.9), channel_id=1, source_target_pairs={{0,8},{4,12},{8,0},{12,4},{16,24},{20,28},{24,16},{28,20},{1,9},{5... | collective-permute-start | bytes 2162696 | tf_op jit(solution)/shard_map/ppermute | solution.py:195
  108.4 149.2 %copy-start.4 = (bf16[384,2048]{1,0:T(8,128)(2,1)}, bf16[384,2048]{1,0:T(8,128)(2,1)S(1)}, u32[]{:S(2)}) copy-start(bf16[384,2048]{1,0:T(8,128)(2,1)S(1)} %pad_maximum_fusion.2.xa_ref) | copy-start | bytes 4718596
  108.5 149.2 %collective-permute-start.11 = (bf16[384,2048]{1,0:T(8,128)(2,1)S(1)}, bf16[384,2048]{1,0:T(8,128)(2,1)}, u32[]{:S(2)}, u32[]{:S(2)}) collective-permute-start(bf16[384,2048]{1,0:T(8,128)(2,1)S(1)} %pad_maximum_fusion.2.xa_ref), channel_id=1, source_target_pairs={{0,1},{1,0},{2,3},{3,2},{4,5},{5,4},{6,7},{7,6},{8,9},{9,8},{10,11... | collective-permute-start | bytes 4718600 | tf_op jit(solution)/shard_map/ppermute | solution.py:208
  109.6 83.5 %collective-permute-start.15 = (bf16[1408,256]{1,0:T(8,128)(2,1)}, bf16[1408,256]{1,0:T(8,128)(2,1)S(1)}, u32[]{:S(2)}, u32[]{:S(2)}) collective-permute-start(bf16[1408,256]{1,0:T(8,128)(2,1)} %pad_maximum_fusion.8.rest_0_), channel_id=1, source_target_pairs={{0,16},{4,20},{8,24},{12,28},{16,0},{20,4},{24,8},{28,12},{1,17},{... | collective-permute-start | bytes 2162696 | tf_op jit(solution)/shard_map/ppermute | solution.py:195
  110.5 83.5 %collective-permute-start.17 = (bf16[1408,256]{1,0:T(8,128)(2,1)S(1)}, bf16[1408,256]{1,0:T(8,128)(2,1)}, u32[]{:S(2)}, u32[]{:S(2)}) collective-permute-start(bf16[1408,256]{1,0:T(8,128)(2,1)S(1)} %pad_maximum_fusion.9), channel_id=1, source_target_pairs={{0,24},{4,28},{8,16},{12,20},{16,8},{20,12},{24,0},{28,4},{1,25},{... | collective-permute-start | bytes 2162696 | tf_op jit(solution)/shard_map/ppermute | solution.py:195
  112.0 79.1 %collective-permute-start.26 = (bf16[704,256]{1,0:T(8,128)(2,1)}, bf16[704,256]{1,0:T(8,128)(2,1)}, u32[]{:S(2)}, u32[]{:S(2)}) collective-permute-start(bf16[704,256]{1,0:T(8,128)(2,1)} %get-tuple-element.18), channel_id=1, source_target_pairs={{0,16},{4,20},{8,24},{12,28},{16,0},{20,4},{24,8},{28,12},{1,17},{... | collective-permute-start | bytes 1081352 | tf_op jit(solution)/shard_map/ppermute | solution.py:195
  191.1 19.3 %collective-permute-start.12 = (bf16[1408,256]{1,0:T(8,128)(2,1)}, bf16[1408,256]{1,0:T(8,128)(2,1)}, u32[]{:S(2)}, u32[]{:S(2)}) collective-permute-start(bf16[1408,256]{1,0:T(8,128)(2,1)} %pad_maximum_fusion.8.rest_0_), channel_id=1, source_target_pairs={{0,4},{4,0},{8,12},{12,8},{16,20},{20,16},{24,28},{28,24},{1,5},{5... | collective-permute-start | bytes 2162696 | tf_op jit(solution)/shard_map/ppermute | solution.py:195
  192.0 33.8 %collective-permute-start.14 = (bf16[1408,256]{1,0:T(8,128)(2,1)}, bf16[1408,256]{1,0:T(8,128)(2,1)}, u32[]{:S(2)}, u32[]{:S(2)}) collective-permute-start(bf16[1408,256]{1,0:T(8,128)(2,1)} %collective-permute-done.13.rest_2_), channel_id=1, source_target_pairs={{0,4},{4,0},{8,12},{12,8},{16,20},{20,16},{24,28},{28,24},{1,5},{5... | collective-permute-start | bytes 2162696 | tf_op jit(solution)/shard_map/ppermute | solution.py:195
  193.1 64.6 %copy-start.18 = (bf16[1408,256]{1,0:T(8,128)(2,1)}, bf16[1408,256]{1,0:T(8,128)(2,1)S(1)}, u32[]{:S(2)}) copy-start(bf16[1408,256]{1,0:T(8,128)(2,1)S(1)} %collective-permute-done.15.rest_4_) | copy-start | bytes 2162692
  193.1 48.2 %collective-permute-start.16 = (bf16[1408,256]{1,0:T(8,128)(2,1)S(1)}, bf16[1408,256]{1,0:T(8,128)(2,1)}, u32[]{:S(2)}, u32[]{:S(2)}) collective-permute-start(bf16[1408,256]{1,0:T(8,128)(2,1)S(1)} %collective-permute-done.15.rest_4_), channel_id=1, source_target_pairs={{0,4},{4,0},{8,12},{12,8},{16,20},{20,16},{24,28},{28,24},{1,5},{5... | collective-permute-start | bytes 2162696 | tf_op jit(solution)/shard_map/ppermute | solution.py:195
  194.1 62.7 %collective-permute-start.18 = (bf16[1408,256]{1,0:T(8,128)(2,1)}, bf16[1408,256]{1,0:T(8,128)(2,1)}, u32[]{:S(2)}, u32[]{:S(2)}) collective-permute-start(bf16[1408,256]{1,0:T(8,128)(2,1)} %collective-permute-done.17.rest_6_), channel_id=1, source_target_pairs={{0,4},{4,0},{8,12},{12,8},{16,20},{20,16},{24,28},{28,24},{1,5},{5... | collective-permute-start | bytes 2162696 | tf_op jit(solution)/shard_map/ppermute | solution.py:195
  210.4 85.6 %collective-permute-start.20 = (bf16[704,256]{1,0:T(8,128)(2,1)}, bf16[704,256]{1,0:T(8,128)(2,1)}, u32[]{:S(2)}, u32[]{:S(2)}) collective-permute-start(bf16[704,256]{1,0:T(8,128)(2,1)} %get-tuple-element.18), channel_id=1, source_target_pairs={{0,4},{4,0},{8,12},{12,8},{16,20},{20,16},{24,28},{28,24},{1,5},{5... | collective-permute-start | bytes 1081352 | tf_op jit(solution)/shard_map/ppermute | solution.py:195
  225.8 54.7 %collective-permute-start.29 = (bf16[704,256]{1,0:T(8,128)(2,1)}, bf16[704,256]{1,0:T(8,128)(2,1)S(1)}, u32[]{:S(2)}, u32[]{:S(2)}) collective-permute-start(bf16[704,256]{1,0:T(8,128)(2,1)} %collective-permute-done.27), channel_id=1, source_target_pairs={{0,4},{4,0},{8,12},{12,8},{16,20},{20,16},{24,28},{28,24},{1,5},{5... | collective-permute-start | bytes 1081352 | tf_op jit(solution)/shard_map/ppermute | solution.py:195
  241.3 39.7 %collective-permute-start.28 = (bf16[704,256]{1,0:T(8,128)(2,1)}, bf16[704,256]{1,0:T(8,128)(2,1)}, u32[]{:S(2)}, u32[]{:S(2)}) collective-permute-start(bf16[704,256]{1,0:T(8,128)(2,1)} %collective-permute-done.26), channel_id=1, source_target_pairs={{0,4},{4,0},{8,12},{12,8},{16,20},{20,16},{24,28},{28,24},{1,5},{5... | collective-permute-start | bytes 1081352 | tf_op jit(solution)/shard_map/ppermute | solution.py:195
  256.7 40.7 %collective-permute-start.21 = (bf16[704,256]{1,0:T(8,128)(2,1)}, bf16[704,256]{1,0:T(8,128)(2,1)}, u32[]{:S(2)}, u32[]{:S(2)}) collective-permute-start(bf16[704,256]{1,0:T(8,128)(2,1)} %collective-permute-done.19), channel_id=1, source_target_pairs={{0,4},{4,0},{8,12},{12,8},{16,20},{20,16},{24,28},{28,24},{1,5},{5... | collective-permute-start | bytes 1081352 | tf_op jit(solution)/shard_map/ppermute | solution.py:195
  274.0 2.1 copy-start.2
  300.2 3.3 copy-start.3
  300.2 3.3 copy-start.17
  306.7 2.4 collective-permute-start.22
  306.9 6.0 %collective-permute-start.30 = (bf16[4,384,256]{2,1,0:T(8,128)(2,1)S(1)}, bf16[4,384,256]{2,1,0:T(8,128)(2,1)S(1)}, u32[]{:S(2)}, u32[]{:S(2)}) collective-permute-start(bf16[4,384,256]{2,1,0:T(8,128)(2,1)S(1)} %fusion.6), channel_id=1, source_target_pairs={{0,1},{1,0},{2,3},{3,2},{4,5},{5,4},{6,7},{7,6},{8,9},{9,8},{10,11... | collective-permute-start | bytes 2359304 | tf_op jit(solution)/shard_map/ppermute | solution.py:208
  309.3 8.6 %collective-permute-start.23 = (bf16[4,96,256]{2,1,0:T(8,128)(2,1)S(1)}, bf16[4,96,256]{2,1,0:T(8,128)(2,1)S(1)}, u32[]{:S(2)}, u32[]{:S(2)}) collective-permute-start(bf16[4,96,256]{2,1,0:T(8,128)(2,1)S(1)} %get-tuple-element.12), channel_id=1, source_target_pairs={{0,2},{1,3},{2,0},{3,1},{4,6},{5,7},{6,4},{7,5},{8,10},{9,11},{10,... | collective-permute-start | bytes 589832 | tf_op jit(solution)/shard_map/ppermute | solution.py:205
  310.9 7.8 %collective-permute-start.24 = (bf16[4,96,256]{2,1,0:T(8,128)(2,1)S(1)}, bf16[4,96,256]{2,1,0:T(8,128)(2,1)S(1)}, u32[]{:S(2)}, u32[]{:S(2)}) collective-permute-start(bf16[4,96,256]{2,1,0:T(8,128)(2,1)S(1)} %get-tuple-element.14), channel_id=1, source_target_pairs={{0,8},{1,9},{2,10},{3,11},{4,12},{5,13},{6,14},{7,15},{8,0},{9,1},... | collective-permute-start | bytes 589832 | tf_op jit(solution)/shard_map/ppermute | solution.py:205
  310.9 12.0 %collective-permute-start.25 = (bf16[4,96,256]{2,1,0:T(8,128)(2,1)S(1)}, bf16[4,96,256]{2,1,0:T(8,128)(2,1)S(1)}, u32[]{:S(2)}, u32[]{:S(2)}) collective-permute-start(bf16[4,96,256]{2,1,0:T(8,128)(2,1)S(1)} %get-tuple-element.13), channel_id=1, source_target_pairs={{0,10},{1,11},{2,8},{3,9},{4,14},{5,15},{6,12},{7,13},{8,2},{9,3},... | collective-permute-start | bytes 589832 | tf_op jit(solution)/shard_map/ppermute | solution.py:205
  313.2 11.6 %collective-permute-start.31 = (bf16[4,96,256]{2,1,0:T(8,128)(2,1)S(1)}, bf16[4,96,256]{2,1,0:T(8,128)(2,1)S(1)}, u32[]{:S(2)}, u32[]{:S(2)}) collective-permute-start(bf16[4,96,256]{2,1,0:T(8,128)(2,1)S(1)} %get-tuple-element.15), channel_id=1, source_target_pairs={{0,2},{1,3},{2,0},{3,1},{4,6},{5,7},{6,4},{7,5},{8,10},{9,11},{10,... | collective-permute-start | bytes 589832 | tf_op jit(solution)/shard_map/ppermute | solution.py:205
  314.8 12.4 %collective-permute-start.32 = (bf16[4,96,256]{2,1,0:T(8,128)(2,1)S(1)}, bf16[4,96,256]{2,1,0:T(8,128)(2,1)S(1)}, u32[]{:S(2)}, u32[]{:S(2)}) collective-permute-start(bf16[4,96,256]{2,1,0:T(8,128)(2,1)S(1)} %get-tuple-element.17), channel_id=1, source_target_pairs={{0,8},{1,9},{2,10},{3,11},{4,12},{5,13},{6,14},{7,15},{8,0},{9,1},... | collective-permute-start | bytes 589832 | tf_op jit(solution)/shard_map/ppermute | solution.py:205
  317.9 12.3 %collective-permute-start.33 = (bf16[4,96,256]{2,1,0:T(8,128)(2,1)S(1)}, bf16[4,96,256]{2,1,0:T(8,128)(2,1)S(1)}, u32[]{:S(2)}, u32[]{:S(2)}) collective-permute-start(bf16[4,96,256]{2,1,0:T(8,128)(2,1)S(1)} %get-tuple-element.16), channel_id=1, source_target_pairs={{0,10},{1,11},{2,8},{3,9},{4,14},{5,15},{6,12},{7,13},{8,2},{9,3},... | collective-permute-start | bytes 589832 | tf_op jit(solution)/shard_map/ppermute | solution.py:205
  330.3 0.7 copy-start.16
  331.9 1.3 copy-start.12
  333.2 0.7 copy-start.13
  333.5 1.5 copy-start.1
